TPU v7x, 32 devices: a whole 2x2x4 slice. The times are simulated.
32 devices in a mesh: sp: 16 (over z, y, core), tp: 2 (over x).
Axes of the slice: x: 2, y: 2, z: 4, core: 2. Of those that a mesh axis runs over, the one named last changes fastest.
Arguments:
- tokens: bfloat16 [16384, 2048], P('sp'), may hold values from -6 to 6
- norm_gain: float32 [2048], replicated, may hold values from 0.1 to 1.9
- w_query: bfloat16 [2048, 512], P(None, 'tp'), may hold values from -0.79549513 to 0.79549513
- w_key: bfloat16 [2048, 128], P('sp'), may hold values from -0.79549513 to 0.79549513
- w_value: bfloat16 [2048, 128], P('sp'), may hold values from -0.125 to 0.125
- w_pool_in: bfloat16 [2048, 512], P(None, 'tp'), may hold values from -0.125 to 0.125
- sink_logit: float32 [8], P('tp'), may hold values from 3 to 7
- pool_scale: float32 [512], P('tp'), may hold values from 0.05 to 0.5
- w_out: bfloat16 [1024, 2048], P('tp', 'sp'), may hold values from -0.75 to 0.75
Outputs:
- mixed_out: bfloat16 [16384, 2048], P(('sp', 'tp'))
All inputs are finite; a program needn't handle non-finite values.
Results may differ from a plain program's by a relative error of at most 0.03.
The roundings to bfloat16 on the way count: a program that leaves them out, or rounds other values in their place, can miss the bound.
Values may be sent and summed in bfloat16 or wider, within the bound.
A program may use at most 64 MiB of HBM per device.

v0:
```python
import jax
import jax.numpy as jnp
from jax import lax
from jax.sharding import PartitionSpec as P

HEAD = 64
QH = 8
KVH = 2
POOL_CH = 128
WINDOW = 128
QB = 128


NEG_BIG = -1e30
POOL_SPANS = (2, 4, 8, 16)


def extended(block, sides, width):
    for axis, dim in sides:
        count = lax.axis_size(axis)
        forward = [(i, i + 1) for i in range(count - 1)]
        backward = [(target, source) for source, target in forward]
        low = lax.ppermute(
            lax.slice_in_dim(block, block.shape[dim] - width, None, axis=dim), axis, forward
        )
        high = lax.ppermute(lax.slice_in_dim(block, 0, width, axis=dim), axis, backward)
        block = jnp.concatenate([low, block, high], axis=dim)
    return block


def layer_normed(tokens, norm_gain):
    values = tokens.astype(jnp.float32)
    center = jnp.mean(values, axis=-1, keepdims=True)
    spread = jnp.mean(jnp.square(values - center), axis=-1, keepdims=True)
    return ((values - center) * lax.rsqrt(spread + 1e-06) * norm_gain).astype(jnp.bfloat16)


def rotate(values, positions):
    half = HEAD // 2
    inverse = 10000.0 ** (-jnp.arange(half, dtype=jnp.float32) / half)
    angles = positions[:, None] * inverse[None, :]
    cosine = jnp.cos(angles)[:, None, :]
    sine = jnp.sin(angles)[:, None, :]
    first = values[..., :half]
    second = values[..., half:]
    return jnp.concatenate(
        [first * cosine - second * sine, first * sine + second * cosine], axis=-1
    )


def body(tokens, norm_gain, w_query, w_key, w_value, w_pool_in, sink_logit, pool_scale, w_out):
    local_rows = tokens.shape[0]
    seq_total = local_rows * lax.axis_size("sp")
    offset = lax.axis_index("sp") * local_rows
    tp_place = lax.axis_index("tp")
    local_heads = w_query.shape[1] // HEAD
    local_pool = w_pool_in.shape[1]
    reach = POOL_SPANS[-1] // 2
    normed = layer_normed(tokens, norm_gain)
    positions = (offset + jnp.arange(local_rows)).astype(jnp.float32)
    query = rotate(
        jnp.dot(normed, w_query, preferred_element_type=jnp.float32).reshape(
            local_rows, local_heads, HEAD
        ),
        positions,
    ).astype(jnp.bfloat16)
    key_head = tp_place * local_heads // (QH // KVH)
    key_cols = lax.dynamic_slice_in_dim(w_key, key_head * HEAD, HEAD, 1)
    value_cols = lax.dynamic_slice_in_dim(w_value, key_head * HEAD, HEAD, 1)
    key_sum = jnp.dot(
        normed,
        lax.all_gather(key_cols, "sp", axis=0, tiled=True),
        preferred_element_type=jnp.float32,
    )
    value_sum = jnp.dot(
        normed,
        lax.all_gather(value_cols, "sp", axis=0, tiled=True),
        preferred_element_type=jnp.float32,
    )
    key = rotate(key_sum[:, None, :], positions)[:, 0, :].astype(jnp.bfloat16)
    value = value_sum.astype(jnp.bfloat16)
    key_value = jnp.concatenate([key, value], axis=1)
    pool_in = jnp.dot(normed, w_pool_in, preferred_element_type=jnp.float32).astype(jnp.bfloat16)
    widened = extended(jnp.concatenate([key_value, pool_in], axis=1), (("sp", 0),), WINDOW)
    kv_wide = widened[:, : 2 * HEAD]
    pool_wide = widened[WINDOW - reach : WINDOW + local_rows + reach, 2 * HEAD :]
    span = QB + 2 * WINDOW
    sink_here = sink_logit[:, None, None]
    results = []
    for block in range(local_rows // QB):
        queries = query[block * QB : (block + 1) * QB]
        keys = kv_wide[block * QB : block * QB + span, :HEAD]
        values = kv_wide[block * QB : block * QB + span, HEAD:]
        scores = jnp.einsum(
            "ihd,jd->hij", queries, keys, preferred_element_type=jnp.float32
        ) * HEAD ** (-0.5)
        query_pos = offset + block * QB + jnp.arange(QB)
        key_pos = offset + block * QB - WINDOW + jnp.arange(span)
        valid = (
            (jnp.abs(query_pos[:, None] - key_pos[None, :]) <= WINDOW)
            & (key_pos[None, :] >= 0)
            & (key_pos[None, :] < seq_total)
        )
        scores = jnp.where(valid, scores, NEG_BIG)
        highest = jnp.maximum(jnp.max(scores, axis=-1, keepdims=True), sink_here)
        expo = jnp.where(valid, jnp.exp(scores - highest), 0.0)
        total = jnp.sum(expo, axis=-1, keepdims=True) + jnp.exp(sink_here - highest)
        weights = (expo / total).astype(jnp.bfloat16)
        result = jnp.einsum("hij,jd->ihd", weights, values, preferred_element_type=jnp.float32)
        results.append(result.reshape(QB, local_heads * HEAD).astype(jnp.bfloat16))
    attended = jnp.concatenate(results, axis=0)
    pool_vals = pool_wide.astype(jnp.float32)
    window_sum = pool_vals
    global_pos = offset + jnp.arange(local_rows)
    channel = tp_place * local_pool + jnp.arange(local_pool)
    window_group = channel // POOL_CH
    measured = jnp.zeros((local_rows, local_pool), jnp.float32)
    stride = 1
    for index, width in enumerate(POOL_SPANS):
        window_sum = window_sum[:-stride] + window_sum[stride:]
        stride = width
        sums = window_sum[reach - width // 2 : reach - width // 2 + local_rows]
        counted = (
            jnp.minimum(global_pos + width // 2, seq_total)
            - jnp.maximum(global_pos - width // 2, 0)
        ).astype(jnp.float32)
        measured = measured + jnp.where(
            window_group[None, :] == index, sums / counted[:, None], 0.0
        )
    pooled = ((measured - pool_vals[reach : reach + local_rows]) * pool_scale).astype(jnp.bfloat16)
    attended_rows, pooled_rows = (
        lax.all_to_all(attended, "tp", split_axis=0, concat_axis=1, tiled=True),
        lax.all_to_all(pooled, "tp", split_axis=0, concat_axis=1, tiled=True),
    )
    joined = jnp.concatenate([attended_rows, pooled_rows], axis=1)
    out_rows_all = lax.all_gather(w_out, "tp", axis=0, tiled=True)
    projected = jnp.dot(
        joined,
        lax.all_gather(out_rows_all, "sp", axis=1, tiled=True),
        preferred_element_type=jnp.float32,
    )
    return projected.astype(jnp.bfloat16)


def solution(mesh):
    in_specs = (
        P("sp", None),
        P(),
        P(None, "tp"),
        P("sp", None),
        P("sp", None),
        P(None, "tp"),
        P("tp"),
        P("tp"),
        P("tp", "sp"),
    )
    out_specs = P(("sp", "tp"), None)
    return jax.shard_map(body, mesh=mesh, in_specs=in_specs, out_specs=out_specs, check_vma=False)
```

profile of v0, /device:TPU:0, one launch (start us, length us, event | category | flops | bytes accessed | tf_op | source)
XLA Modules:
  0.0 166.7 jit_solution(2030448479956947112)
XLA Ops:
  6.6 0.9 constant_dynamic-slice_fusion.1
  7.5 24.6 %all_gather.12 = bf16[2048,64]{1,0:T(8,128)(2,1)S(1)} all-gather(bf16[128,64]{1,0:T(8,128)(2,1)S(1)} %constant_dynamic-slice_fusion.1), channel_id=1, replica_groups=mesh['sp'=16,'tp'=2] {'sp'}, dimensions={0}, use_global_device_ids=true | all-gather | bytes 278528 | tf_op jit(solution)/shard_map/all_gather | solution.py:72
  32.1 3.0 %convert_reduce_fusion = f32[1024]{0:T(1024)S(1)} fusion(bf16[1024,2048]{1,0:T(8,128)(2,1)} %param.9), kind=kLoop, calls=%fused_computation.1 | loop fusion | flops 4193280 | bytes 4198400 | tf_op jit(solution)/shard_map/reduce_sum | solution.py:33
  35.1 0.5 copy-done.1
  35.5 1.2 fusion.2
  36.9 18.9 %all_gather.13 = bf16[2048,64]{1,0:T(8,128)(2,1)S(1)} all-gather(bf16[128,64]{1,0:T(8,128)(2,1)S(1)} %constant_dynamic-slice_fusion), channel_id=1, replica_groups=mesh['sp'=16,'tp'=2] {'sp'}, dimensions={0}, use_global_device_ids=true | all-gather | bytes 278528 | tf_op jit(solution)/shard_map/all_gather | solution.py:77
  55.8 3.0 %fusion.4 = bf16[1024,2048]{1,0:T(8,128)(2,1)S(1)} fusion(bf16[1024,2048]{1,0:T(8,128)(2,1)} %param.9, f32[2048]{0:T(1024)S(1)} %copy-done.53, f32[1024]{0:T(1024)S(1)} %add_rsqrt_fusion, f32[1024]{0:T(1024)S(1)} %broadcast_multiply_fusion), kind=kLoop, calls=%fused_computation.6 | loop fusion | flops 10485760 | bytes 8404992 | tf_op jit(solution)/shard_map/convert_element_type | solution.py:35
  58.8 1.4 convolution_bitcast_fusion
  60.2 1.4 convolution_convert_fusion.2
  61.6 1.3 convolution_convert_fusion.1
  62.9 0.6 fusion.64
  63.6 1.3 collective-permute-start.1
  64.9 3.7 %collective-permute-start = (bf16[128,384]{0,1:T(8,128)(2,1)S(1)}, bf16[128,384]{0,1:T(8,128)(2,1)}, u32[]{:S(2)}, u32[]{:S(2)}) collective-permute-start(bf16[128,384]{0,1:T(8,128)(2,1)S(1)} %get-tuple-element.9), channel_id=1, source_target_pairs={{0,2},{2,4},{4,6},{6,8},{8,10},{10,12},{12,14},{14,16},{16,18},{18... | collective-permute-start | bytes 294920 | tf_op jit(solution)/shard_map/ppermute | solution.py:23
  68.5 7.3 %all_gather.14 = bf16[1024,128]{1,0:T(8,128)(2,1)} all-gather(bf16[512,128]{1,0:T(8,128)(2,1)S(1)} %copy-done.28), channel_id=1, replica_groups=mesh['sp'=16,'tp'=2] {'tp'}, dimensions={0}, use_global_device_ids=true | all-gather | bytes 393216 | tf_op jit(solution)/shard_map/all_gather | solution.py:136
  75.9 0.5 multiply_cosine_fusion
  76.7 0.6 subtract_convert_fusion.1
  77.3 0.6 subtract_convert_fusion.3
  77.9 3.8 %fusion.164 = f32[1024,256]{0,1:T(8,128)S(1)} fusion(bf16[1024,2048]{1,0:T(8,128)(2,1)} %copy-done.2, bf16[2048,256]{1,0:T(8,128)(2,1)} %param.11), kind=kOutput, calls=%fused_computation.317 | convolution fusion | flops 1073741824 | bytes 6291456 | tf_op jit(solution)/shard_map/dot_general | solution.py:62
  82.1 1.7 %fusion.163 = (f32[4,128]{1,0:T(4,128)}, f32[4,128,384]{1,2,0:T(8,128)}) fusion(bf16[1024,4,32]{0,2,1:T(8,128)(2,1)S(1)} %get-tuple-element.6, bf16[1024,4,32]{0,2,1:T(8,128)(2,1)S(1)} %get-tuple-element.5, bf16[1024,1,32]{0,2,1:T(8,128)(2,1)S(1)} %get-tuple-element.11, bf16[1024,1,32]{0,2,1:T(8,128)(2,1)S(1)} %get-tuple-element.12, ...), kind=kOutput, calls=%fused_computation.316 | convolution fusion | flops 25984512 | bytes 1492992 | tf_op jit(solution)/shard_map/ihd,jd->hij/dot_general | solution.py:94
  84.0 1.8 %fusion.162 = (f32[4,128]{1,0:T(4,128)}, f32[4,128,384]{1,2,0:T(8,128)}) fusion(bf16[1024,4,32]{0,2,1:T(8,128)(2,1)S(1)} %get-tuple-element.6, bf16[1024,4,32]{0,2,1:T(8,128)(2,1)S(1)} %get-tuple-element.5, bf16[1024,1,32]{0,2,1:T(8,128)(2,1)S(1)} %get-tuple-element.11, bf16[1024,1,32]{0,2,1:T(8,128)(2,1)S(1)} %get-tuple-element.12, ...), kind=kOutput, calls=%fused_computation.315 | convolution fusion | flops 25984512 | bytes 1492992 | tf_op jit(solution)/shard_map/ihd,jd->hij/dot_general | solution.py:94
  86.1 1.8 %fusion.161 = (f32[4,128]{1,0:T(4,128)}, f32[4,128,384]{1,2,0:T(8,128)}) fusion(bf16[1024,4,32]{0,2,1:T(8,128)(2,1)S(1)} %get-tuple-element.6, bf16[1024,4,32]{0,2,1:T(8,128)(2,1)S(1)} %get-tuple-element.5, bf16[1024,1,32]{0,2,1:T(8,128)(2,1)S(1)} %get-tuple-element.11, bf16[1024,1,32]{0,2,1:T(8,128)(2,1)S(1)} %get-tuple-element.12, ...), kind=kOutput, calls=%fused_computation.314 | convolution fusion | flops 25984512 | bytes 1492992 | tf_op jit(solution)/shard_map/ihd,jd->hij/dot_general | solution.py:94
  88.1 1.8 %fusion.160 = (f32[4,128]{1,0:T(4,128)}, f32[4,128,384]{1,2,0:T(8,128)}) fusion(bf16[1024,4,32]{0,2,1:T(8,128)(2,1)S(1)} %get-tuple-element.6, bf16[1024,4,32]{0,2,1:T(8,128)(2,1)S(1)} %get-tuple-element.5, bf16[1024,1,32]{0,2,1:T(8,128)(2,1)S(1)} %get-tuple-element.11, bf16[1024,1,32]{0,2,1:T(8,128)(2,1)S(1)} %get-tuple-element.12, ...), kind=kOutput, calls=%fused_computation.313 | convolution fusion | flops 25984512 | bytes 1492992 | tf_op jit(solution)/shard_map/ihd,jd->hij/dot_general | solution.py:94
  90.1 1.8 %fusion.159 = (f32[4,128]{1,0:T(4,128)}, f32[4,128,384]{1,2,0:T(8,128)}) fusion(bf16[1024,4,32]{0,2,1:T(8,128)(2,1)S(1)} %get-tuple-element.6, bf16[1024,4,32]{0,2,1:T(8,128)(2,1)S(1)} %get-tuple-element.5, bf16[1024,1,32]{0,2,1:T(8,128)(2,1)S(1)} %get-tuple-element.11, bf16[1024,1,32]{0,2,1:T(8,128)(2,1)S(1)} %get-tuple-element.12, ...), kind=kOutput, calls=%fused_computation.312 | convolution fusion | flops 25984512 | bytes 1492992 | tf_op jit(solution)/shard_map/ihd,jd->hij/dot_general | solution.py:94
  92.1 1.7 %fusion.158 = (f32[4,128]{1,0:T(4,128)}, f32[4,128,384]{1,2,0:T(8,128)}) fusion(bf16[1024,4,32]{0,2,1:T(8,128)(2,1)S(1)} %get-tuple-element.6, bf16[1024,4,32]{0,2,1:T(8,128)(2,1)S(1)} %get-tuple-element.5, bf16[1024,1,32]{0,2,1:T(8,128)(2,1)S(1)} %get-tuple-element.11, bf16[1024,1,32]{0,2,1:T(8,128)(2,1)S(1)} %get-tuple-element.12, ...), kind=kOutput, calls=%fused_computation.311 | convolution fusion | flops 25984512 | bytes 1492992 | tf_op jit(solution)/shard_map/ihd,jd->hij/dot_general | solution.py:94
  93.8 0.6 broadcast_compare_fusion
  94.9 0.6 broadcast_compare_fusion.2
  95.8 1.0 fusion.157
  97.1 0.4 copy-done.46
  97.8 0.7 exponential_add_fusion
  98.4 1.6 convolution_convert_fusion.3
  100.1 1.6 copy.42
  101.7 1.0 fusion.39
  102.8 1.3 fusion.38
  104.1 1.0 fusion.37
  105.7 0.7 exponential_add_fusion.1
  106.4 0.9 convolution_convert_fusion.4
  107.3 1.6 copy.41
  108.9 1.6 convolution_convert_fusion.5
  110.5 1.6 copy.40
  112.1 2.1 %convolution_convert_fusion.6 = bf16[64,4,128]{2,0,1:T(8,128)(2,1)} fusion(f32[4,128,384]{1,2,0:T(8,128)} %get-tuple-element.42, f32[4,128]{1,0:T(4,128)} %get-tuple-element.29, f32[4,128]{1,0:T(4,128)} %get-tuple-element.20, pred[128,384]{0,1:T(8,128)(4,1)S(1)} %fusion.52, bf16[1024,64]{0,1:T(8,128)(2,1)S(1)} %convolution_convert_fusion.2), kind=kOutput, calls=%fused_computation.41 | convolution fusion | flops 25985024 | bytes 954368 | tf_op jit(solution)/shard_map/hij,jd->ihd/dot_general | solution.py:109
  114.2 1.6 copy.39
  115.8 1.6 convolution_convert_fusion.7
  117.4 1.6 copy.38
  119.0 2.1 %convolution_convert_fusion.8 = bf16[64,4,128]{2,0,1:T(8,128)(2,1)} fusion(f32[4,128,384]{1,2,0:T(8,128)} %get-tuple-element.38, f32[4,128]{1,0:T(4,128)S(1)} %copy-done.58, f32[4,128]{1,0:T(4,128)S(1)} %copy-done.51, pred[128,384]{0,1:T(8,128)(4,1)S(1)} %copy-done.14, bf16[1024,64]{0,1:T(8,128)(2,1)S(1)} %convolution_convert_fusion.2), kind=kOutput, calls=%fused_computation.43 | convolution fusion | flops 25985024 | bytes 954368 | tf_op jit(solution)/shard_map/hij,jd->ihd/dot_general | solution.py:109
  121.1 1.6 copy.37
  122.7 0.9 convolution_convert_fusion.9
  123.6 1.0 copy.36
  124.7 1.1 convolution_convert_fusion.10
  125.9 0.6 constant_dynamic-update-slice_fusion.7
  126.5 0.6 constant_dynamic-update-slice_fusion.6
  127.2 0.6 constant_dynamic-update-slice_fusion.5
  127.8 0.6 constant_dynamic-update-slice_fusion.4
  128.4 0.6 constant_dynamic-update-slice_fusion.3
  129.0 0.6 constant_dynamic-update-slice_fusion.2
  129.7 0.6 constant_dynamic-update-slice_fusion.1
  130.3 0.6 constant_dynamic-update-slice_fusion
  130.9 3.7 %all-to-all-start = ((bf16[2,512,256]{2,1,0:T(8,128)(2,1)}), bf16[2,512,256]{2,1,0:T(8,128)(2,1)S(1)}, u32[]{:S(2)}, u32[]{:S(2)}) async-start(bf16[2,512,256]{2,1,0:T(8,128)(2,1)} %bitcast.49), calls=%async_computation | async-start | bytes 1048576 | tf_op jit(solution)/shard_map/all_to_all | solution.py:132
  134.6 1.1 fusion.42
  137.7 1.6 fusion.22
  139.3 0.8 copy.55
  140.2 2.7 %all-to-all-done = bf16[2,512,256]{2,1,0:T(8,128)(2,1)S(1)} async-done(((bf16[2,512,256]{2,1,0:T(8,128)(2,1)}), bf16[2,512,256]{2,1,0:T(8,128)(2,1)S(1)}, u32[]{:S(2)}, u32[]{:S(2)}) %all-to-all-start) | async-done | bytes 524320 | tf_op jit(solution)/shard_map/all_to_all | solution.py:132
  142.9 3.5 %all-to-all-start.1 = ((bf16[2,512,256]{1,2,0:T(8,128)(2,1)}), bf16[2,512,256]{1,2,0:T(8,128)(2,1)S(1)}, u32[]{:S(2)}, u32[]{:S(2)}) async-start(bf16[2,512,256]{1,2,0:T(8,128)(2,1)} %bitcast.149), calls=%async_computation.1 | async-start | bytes 1048576 | tf_op jit(solution)/shard_map/all_to_all | solution.py:133
  146.6 7.4 %all-to-all-done.1 = bf16[2,512,256]{1,2,0:T(8,128)(2,1)S(1)} async-done(((bf16[2,512,256]{1,2,0:T(8,128)(2,1)}), bf16[2,512,256]{1,2,0:T(8,128)(2,1)S(1)}, u32[]{:S(2)}, u32[]{:S(2)}) %all-to-all-start.1) | async-done | bytes 524320 | tf_op jit(solution)/shard_map/all_to_all | solution.py:133
  154.0 5.9 %convolution_convert_fusion = bf16[512,2048]{1,0:T(8,128)(2,1)} fusion(bf16[1024,2048]{1,0:T(8,128)(2,1)} %all-gather.2.cloned.1.call-done, bf16[512,512]{0,1:T(8,128)(2,1)S(1)} %bitcast.153, bf16[512,512]{0,1:T(8,128)(2,1)S(1)} %bitcast.154), kind=kOutput, calls=%fused_computation.7 | convolution fusion | flops 2150629376 | bytes 7340032 | tf_op jit(solution)/shard_map/dot_general | solution.py:137
  (184 shorter events, 5.7 us)
Async XLA Ops:
  6.5 55.1 %copy-start = (bf16[2048,256]{1,0:T(8,128)(2,1)S(1)}, bf16[2048,256]{1,0:T(8,128)(2,1)}, u32[]{:S(2)}) copy-start(bf16[2048,256]{1,0:T(8,128)(2,1)} %param.14) | copy-start | bytes 3145732
  6.5 147.5 %all-gather.2.cloned.1.call-start = ((), (), s32[]{:S(2)}) async-start(), calls=%async_computation.2 | async-start | bytes 4456448 | tf_op jit(solution)/shard_map/all_gather | solution.py:139
  32.1 3.4 %copy-start.1 = (bf16[1024,2048]{1,0:T(8,128)(2,1)S(1)}, bf16[1024,2048]{1,0:T(8,128)(2,1)}, u32[]{:S(2)}) copy-start(bf16[1024,2048]{1,0:T(8,128)(2,1)} %param.9) | copy-start | bytes 12582916
  35.5 1.3 copy-start.29
  35.5 20.2 %copy-start.53 = (f32[2048]{0:T(1024)S(1)}, f32[2048]{0:T(1024)}, u32[]{:S(2)}) copy-start(f32[2048]{0:T(1024)} %param.10) | copy-start | bytes 24580
  58.8 2.8 %copy-start.2 = (bf16[1024,2048]{1,0:T(8,128)(2,1)}, bf16[1024,2048]{1,0:T(8,128)(2,1)S(1)}, u32[]{:S(2)}) copy-start(bf16[1024,2048]{1,0:T(8,128)(2,1)S(1)} %fusion.4) | copy-start | bytes 12582916
  61.6 6.9 %copy-start.28 = (bf16[512,128]{1,0:T(8,128)(2,1)S(1)}, bf16[512,128]{1,0:T(8,128)(2,1)}, u32[]{:S(2)}) copy-start(bf16[512,128]{1,0:T(8,128)(2,1)} %param.17) | copy-start | bytes 393220
  63.6 31.9 %collective-permute-start.1 = (bf16[128,384]{0,1:T(8,128)(2,1)S(1)}, bf16[128,384]{0,1:T(8,128)(2,1)S(1)}, u32[]{:S(2)}, u32[]{:S(2)}) collective-permute-start(bf16[128,384]{0,1:T(8,128)(2,1)S(1)} %get-tuple-element.10), channel_id=1, source_target_pairs={{2,0},{4,2},{6,4},{8,6},{10,8},{12,10},{14,12},{16,14},{18,16},{20... | collective-permute-start | bytes 294920 | tf_op jit(solution)/shard_map/ppermute | solution.py:26
  64.9 31.0 %collective-permute-start = (bf16[128,384]{0,1:T(8,128)(2,1)S(1)}, bf16[128,384]{0,1:T(8,128)(2,1)}, u32[]{:S(2)}, u32[]{:S(2)}) collective-permute-start(bf16[128,384]{0,1:T(8,128)(2,1)S(1)} %get-tuple-element.9), channel_id=1, source_target_pairs={{0,2},{2,4},{4,6},{6,8},{8,10},{10,12},{12,14},{14,16},{16,18},{18... | collective-permute-start | bytes 294920 | tf_op jit(solution)/shard_map/ppermute | solution.py:23
  88.1 5.7 %copy-start.10 = (pred[128,384]{0,1:T(8,128)(4,1)}, pred[128,384]{0,1:T(8,128)(4,1)S(1)}, u32[]{:S(2)}) copy-start(pred[128,384]{0,1:T(8,128)(4,1)S(1)} %fusion.50) | copy-start | bytes 147460
  90.1 5.7 %copy-start.12 = (pred[128,384]{0,1:T(8,128)(4,1)}, pred[128,384]{0,1:T(8,128)(4,1)S(1)}, u32[]{:S(2)}) copy-start(pred[128,384]{0,1:T(8,128)(4,1)S(1)} %fusion.48) | copy-start | bytes 147460
  92.1 4.8 %copy-start.15 = (pred[128,384]{0,1:T(8,128)(4,1)}, pred[128,384]{0,1:T(8,128)(4,1)S(1)}, u32[]{:S(2)}) copy-start(pred[128,384]{0,1:T(8,128)(4,1)S(1)} %fusion.46) | copy-start | bytes 147460
  94.8 2.1 %copy-start.18 = (pred[128,384]{0,1:T(8,128)(4,1)}, pred[128,384]{0,1:T(8,128)(4,1)S(1)}, u32[]{:S(2)}) copy-start(pred[128,384]{0,1:T(8,128)(4,1)S(1)} %fusion.44) | copy-start | bytes 147460
  95.5 1.4 copy-start.54
  95.5 1.4 copy-start.20
  95.8 1.9 %copy-start.30 = (f32[4,128]{1,0:T(4,128)S(1)}, f32[4,128]{1,0:T(4,128)}, u32[]{:S(2)}) copy-start(f32[4,128]{1,0:T(4,128)} %get-tuple-element.45) | copy-start | bytes 6148
  95.8 1.9 %copy-start.32 = (f32[4,128]{1,0:T(4,128)S(1)}, f32[4,128]{1,0:T(4,128)}, u32[]{:S(2)}) copy-start(f32[4,128]{1,0:T(4,128)} %get-tuple-element.43) | copy-start | bytes 6148
  95.8 1.9 %copy-start.34 = (f32[4,128]{1,0:T(4,128)S(1)}, f32[4,128]{1,0:T(4,128)}, u32[]{:S(2)}) copy-start(f32[4,128]{1,0:T(4,128)} %get-tuple-element.41) | copy-start | bytes 6148
  95.8 1.9 %copy-start.36 = (f32[4,128]{1,0:T(4,128)S(1)}, f32[4,128]{1,0:T(4,128)}, u32[]{:S(2)}) copy-start(f32[4,128]{1,0:T(4,128)} %get-tuple-element.39) | copy-start | bytes 6148
  95.8 1.9 %copy-start.38 = (f32[4,128]{1,0:T(4,128)S(1)}, f32[4,128]{1,0:T(4,128)}, u32[]{:S(2)}) copy-start(f32[4,128]{1,0:T(4,128)} %get-tuple-element.37) | copy-start | bytes 6148
  95.8 1.9 %copy-start.40 = (f32[4,128]{1,0:T(4,128)S(1)}, f32[4,128]{1,0:T(4,128)}, u32[]{:S(2)}) copy-start(f32[4,128]{1,0:T(4,128)} %get-tuple-element.35) | copy-start | bytes 6148
  97.7 4.0 %copy-start.4 = (f32[4,128,384]{1,2,0:T(8,128)S(1)}, f32[4,128,384]{1,2,0:T(8,128)}, u32[]{:S(2)}) copy-start(f32[4,128,384]{1,2,0:T(8,128)} %get-tuple-element.44) | copy-start | bytes 2359300
  101.6 2.5 %copy-start.5 = (f32[4,128,384]{1,2,0:T(8,128)S(1)}, f32[4,128,384]{1,2,0:T(8,128)}, u32[]{:S(2)}) copy-start(f32[4,128,384]{1,2,0:T(8,128)} %get-tuple-element.40) | copy-start | bytes 2359300
  101.6 3.4 %copy-start.7 = (f32[4,128,384]{1,2,0:T(8,128)S(1)}, f32[4,128,384]{1,2,0:T(8,128)}, u32[]{:S(2)}) copy-start(f32[4,128,384]{1,2,0:T(8,128)} %get-tuple-element.38) | copy-start | bytes 2359300
  101.6 3.4 %copy-start.13 = (pred[128,384]{0,1:T(8,128)(4,1)S(1)}, pred[128,384]{0,1:T(8,128)(4,1)}, u32[]{:S(2)}) copy-start(pred[128,384]{0,1:T(8,128)(4,1)} %copy-done.12) | copy-start | bytes 147460
  101.7 3.4 %copy-start.50 = (f32[4,128]{1,0:T(4,128)S(1)}, f32[4,128]{1,0:T(4,128)}, u32[]{:S(2)}) copy-start(f32[4,128]{1,0:T(4,128)} %get-tuple-element.18) | copy-start | bytes 6148
  101.7 3.6 %copy-start.8 = (f32[4,128,384]{1,2,0:T(8,128)S(1)}, f32[4,128,384]{1,2,0:T(8,128)}, u32[]{:S(2)}) copy-start(f32[4,128,384]{1,2,0:T(8,128)} %get-tuple-element.36) | copy-start | bytes 2359300
  101.7 3.6 %copy-start.16 = (pred[128,384]{0,1:T(8,128)(4,1)S(1)}, pred[128,384]{0,1:T(8,128)(4,1)}, u32[]{:S(2)}) copy-start(pred[128,384]{0,1:T(8,128)(4,1)} %copy-done.15) | copy-start | bytes 147460
  101.7 3.6 %copy-start.48 = (f32[4,128]{1,0:T(4,128)S(1)}, f32[4,128]{1,0:T(4,128)}, u32[]{:S(2)}) copy-start(f32[4,128]{1,0:T(4,128)} %get-tuple-element.17) | copy-start | bytes 6148
  101.7 3.8 %copy-start.3 = (f32[4,128,384]{1,2,0:T(8,128)S(1)}, f32[4,128,384]{1,2,0:T(8,128)}, u32[]{:S(2)}) copy-start(f32[4,128,384]{1,2,0:T(8,128)} %get-tuple-element.46) | copy-start | bytes 2359300
  101.7 3.8 %copy-start.52 = (f32[4,128]{1,0:T(4,128)S(1)}, f32[4,128]{1,0:T(4,128)}, u32[]{:S(2)}) copy-start(f32[4,128]{1,0:T(4,128)} %get-tuple-element.22) | copy-start | bytes 6148
  102.7 2.9 %copy-start.31 = (f32[4,128]{1,0:T(4,128)S(1)}, f32[4,128]{1,0:T(4,128)}, u32[]{:S(2)}) copy-start(f32[4,128]{1,0:T(4,128)} %get-tuple-element.45) | copy-start | bytes 6148
  102.7 2.9 %copy-start.33 = (f32[4,128]{1,0:T(4,128)S(1)}, f32[4,128]{1,0:T(4,128)}, u32[]{:S(2)}) copy-start(f32[4,128]{1,0:T(4,128)} %get-tuple-element.43) | copy-start | bytes 6148
  102.7 2.9 %copy-start.35 = (f32[4,128]{1,0:T(4,128)S(1)}, f32[4,128]{1,0:T(4,128)}, u32[]{:S(2)}) copy-start(f32[4,128]{1,0:T(4,128)} %get-tuple-element.41) | copy-start | bytes 6148
  102.7 2.9 %copy-start.37 = (f32[4,128]{1,0:T(4,128)S(1)}, f32[4,128]{1,0:T(4,128)}, u32[]{:S(2)}) copy-start(f32[4,128]{1,0:T(4,128)} %get-tuple-element.39) | copy-start | bytes 6148
  102.7 2.9 %copy-start.39 = (f32[4,128]{1,0:T(4,128)S(1)}, f32[4,128]{1,0:T(4,128)}, u32[]{:S(2)}) copy-start(f32[4,128]{1,0:T(4,128)} %get-tuple-element.37) | copy-start | bytes 6148
  102.8 2.9 %copy-start.41 = (f32[4,128]{1,0:T(4,128)S(1)}, f32[4,128]{1,0:T(4,128)}, u32[]{:S(2)}) copy-start(f32[4,128]{1,0:T(4,128)} %get-tuple-element.35) | copy-start | bytes 6148
  102.8 2.9 %copy-start.55 = (f32[4]{0:T(128)S(1)}, f32[4]{0:T(128)}, u32[]{:S(2)}) copy-start(f32[4]{0:T(128)} %param.15) | copy-start | bytes 52
  110.5 5.3 %copy-start.6 = (f32[4,128,384]{1,2,0:T(8,128)S(1)}, f32[4,128,384]{1,2,0:T(8,128)}, u32[]{:S(2)}) copy-start(f32[4,128,384]{1,2,0:T(8,128)} %get-tuple-element.40) | copy-start | bytes 2359300
  110.5 5.3 %copy-start.11 = (pred[128,384]{0,1:T(8,128)(4,1)S(1)}, pred[128,384]{0,1:T(8,128)(4,1)}, u32[]{:S(2)}) copy-start(pred[128,384]{0,1:T(8,128)(4,1)} %copy-done.10) | copy-start | bytes 147460
  114.2 4.8 %copy-start.14 = (pred[128,384]{0,1:T(8,128)(4,1)S(1)}, pred[128,384]{0,1:T(8,128)(4,1)}, u32[]{:S(2)}) copy-start(pred[128,384]{0,1:T(8,128)(4,1)} %copy-done.12) | copy-start | bytes 147460
  114.2 4.8 %copy-start.51 = (f32[4,128]{1,0:T(4,128)S(1)}, f32[4,128]{1,0:T(4,128)}, u32[]{:S(2)}) copy-start(f32[4,128]{1,0:T(4,128)} %get-tuple-element.18) | copy-start | bytes 6148
  114.2 4.8 %copy-start.58 = (f32[4,128]{1,0:T(4,128)S(1)}, f32[4,128]{1,0:T(4,128)}, u32[]{:S(2)}) copy-start(f32[4,128]{1,0:T(4,128)} %get-tuple-element.27) | copy-start | bytes 6148
  117.4 5.3 %copy-start.9 = (f32[4,128,384]{1,2,0:T(8,128)S(1)}, f32[4,128,384]{1,2,0:T(8,128)}, u32[]{:S(2)}) copy-start(f32[4,128,384]{1,2,0:T(8,128)} %get-tuple-element.36) | copy-start | bytes 2359300
  117.4 5.3 %copy-start.17 = (pred[128,384]{0,1:T(8,128)(4,1)S(1)}, pred[128,384]{0,1:T(8,128)(4,1)}, u32[]{:S(2)}) copy-start(pred[128,384]{0,1:T(8,128)(4,1)} %copy-done.15) | copy-start | bytes 147460
  117.4 5.3 %copy-start.49 = (f32[4,128]{1,0:T(4,128)S(1)}, f32[4,128]{1,0:T(4,128)}, u32[]{:S(2)}) copy-start(f32[4,128]{1,0:T(4,128)} %get-tuple-element.17) | copy-start | bytes 6148
  117.4 5.3 %copy-start.57 = (f32[4,128]{1,0:T(4,128)S(1)}, f32[4,128]{1,0:T(4,128)}, u32[]{:S(2)}) copy-start(f32[4,128]{1,0:T(4,128)} %get-tuple-element.26) | copy-start | bytes 6148
  121.1 3.5 %copy-start.19 = (pred[128,384]{0,1:T(8,128)(4,1)S(1)}, pred[128,384]{0,1:T(8,128)(4,1)}, u32[]{:S(2)}) copy-start(pred[128,384]{0,1:T(8,128)(4,1)} %copy-done.18) | copy-start | bytes 147460
  121.1 3.5 %copy-start.47 = (f32[4,128]{1,0:T(4,128)S(1)}, f32[4,128]{1,0:T(4,128)}, u32[]{:S(2)}) copy-start(f32[4,128]{1,0:T(4,128)} %copy-done.46) | copy-start | bytes 6148
  121.1 3.5 %copy-start.56 = (f32[4,128]{1,0:T(4,128)S(1)}, f32[4,128]{1,0:T(4,128)}, u32[]{:S(2)}) copy-start(f32[4,128]{1,0:T(4,128)} %get-tuple-element.16) | copy-start | bytes 6148
  123.6 3.5 %copy-start.27 = (bf16[128,256]{1,0:T(8,128)(2,1)S(1)}, bf16[128,256]{1,0:T(8,128)(2,1)}, u32[]{:S(2)}) copy-start(bf16[128,256]{1,0:T(8,128)(2,1)} %copy.37) | copy-start | bytes 196612
  124.6 3.2 %copy-start.26 = (bf16[128,256]{1,0:T(8,128)(2,1)S(1)}, bf16[128,256]{1,0:T(8,128)(2,1)}, u32[]{:S(2)}) copy-start(bf16[128,256]{1,0:T(8,128)(2,1)} %copy.38) | copy-start | bytes 196612
  124.6 3.8 %copy-start.25 = (bf16[128,256]{1,0:T(8,128)(2,1)S(1)}, bf16[128,256]{1,0:T(8,128)(2,1)}, u32[]{:S(2)}) copy-start(bf16[128,256]{1,0:T(8,128)(2,1)} %copy.39) | copy-start | bytes 196612
  124.6 4.4 %copy-start.24 = (bf16[128,256]{1,0:T(8,128)(2,1)S(1)}, bf16[128,256]{1,0:T(8,128)(2,1)}, u32[]{:S(2)}) copy-start(bf16[128,256]{1,0:T(8,128)(2,1)} %copy.40) | copy-start | bytes 196612
  124.7 5.0 %copy-start.23 = (bf16[128,256]{1,0:T(8,128)(2,1)S(1)}, bf16[128,256]{1,0:T(8,128)(2,1)}, u32[]{:S(2)}) copy-start(bf16[128,256]{1,0:T(8,128)(2,1)} %copy.41) | copy-start | bytes 196612
  124.7 5.6 %copy-start.22 = (bf16[128,256]{1,0:T(8,128)(2,1)S(1)}, bf16[128,256]{1,0:T(8,128)(2,1)}, u32[]{:S(2)}) copy-start(bf16[128,256]{1,0:T(8,128)(2,1)} %copy.42) | copy-start | bytes 196612
  124.7 9.9 %copy-start.21 = (bf16[128,384]{0,1:T(8,128)(2,1)S(1)}, bf16[128,384]{0,1:T(8,128)(2,1)}, u32[]{:S(2)}) copy-start(bf16[128,384]{0,1:T(8,128)(2,1)} %copy-done.20) | copy-start | bytes 294916
  130.9 12.0 %all-to-all-start = ((bf16[2,512,256]{2,1,0:T(8,128)(2,1)}), bf16[2,512,256]{2,1,0:T(8,128)(2,1)S(1)}, u32[]{:S(2)}, u32[]{:S(2)}) async-start(bf16[2,512,256]{2,1,0:T(8,128)(2,1)} %bitcast.49), calls=%async_computation | async-start | bytes 1048576 | tf_op jit(solution)/shard_map/all_to_all | solution.py:132
  136.9 0.7 copy-start.42
  137.0 0.7 copy-start.44
  137.0 0.7 copy-start.45
  137.0 0.7 copy-start.59
  137.0 0.7 copy-start.60
  142.9 11.1 %all-to-all-start.1 = ((bf16[2,512,256]{1,2,0:T(8,128)(2,1)}), bf16[2,512,256]{1,2,0:T(8,128)(2,1)S(1)}, u32[]{:S(2)}, u32[]{:S(2)}) async-start(bf16[2,512,256]{1,2,0:T(8,128)(2,1)} %bitcast.149), calls=%async_computation.1 | async-start | bytes 1048576 | tf_op jit(solution)/shard_map/all_to_all | solution.py:133
  (5 other events, 3.3 us)
Sparse Core Ops, SparseCore 0:
  76.0 49.8 all-gather.1
where the time goes:
time: 168 us; the launch traced here: 167 us
  blocking collectives  50.8 us (30%)
  matrix products  37.6 us (22%)
  other arithmetic  22.2 us (13%)
  local copies, waits for them, and re-layouts  19.4 us (12%)
  between operations  14.5 us (9%)
  starting transfers between devices  12.2 us (7%)
  waiting for transfers between devices  10.2 us (6%)
    all_gather x1, blocking collectives, body(): lax.all_gather(key_cols, 'sp', axis=0, tiled=True)  24.6 us
    all_gather x1, blocking collectives, body(): lax.all_gather(value_cols, 'sp', axis=0, tiled=True)  18.9 us
    dot_general x8, matrix products, body(): jnp.einsum('hij,jd->ihd', weights, values, preferred_element_type=jnp.flo...  11.9 us
    dot_general x8, matrix products, body(): jnp.einsum('ihd,jd->hij', queries, keys, preferred_element_type=jnp.float32)  11.9 us
    convert_element_type x8, local copies, waits for them, and re-layouts, body(): results.append(result.reshape(QB, local_heads * HEAD).astype(jnp.bfloat16))  10.6 us
    all_to_all x1, waiting for transfers between devices, body(): lax.all_to_all(pooled, 'tp', split_axis=0, concat_axis=1, tiled=True)  7.42 us
    all_gather x1, blocking collectives, body(): out_rows_all = lax.all_gather(w_out, 'tp', axis=0, tiled=True)  7.31 us
    dot_general x1, matrix products, body(): jnp.dot(joined, lax.all_gather(out_rows_all, 'sp', axis=1, tiled=True), p...  5.88 us
  transfers between devices with their start and end apart: 5, of which 2 were waited for; matrix products, arithmetic and copies ran while one was open for 35% of the time, Pallas kernels for 0%

commit v1 on v0

--- a/solution.py
+++ b/solution.py
@@ -1,6 +1,10 @@
+import functools
+
 import jax
 import jax.numpy as jnp
 from jax import lax
+from jax.experimental import pallas as pl
+from jax.experimental.pallas import tpu as pltpu
 from jax.sharding import PartitionSpec as P
 
 HEAD = 64
@@ -48,7 +52,7 @@
     )
 
 
-def body(tokens, norm_gain, w_query, w_key, w_value, w_pool_in, sink_logit, pool_scale, w_out):
+def plain_body(tokens, norm_gain, w_query, w_key, w_value, w_pool_in, sink_logit, pool_scale, w_out):
     local_rows = tokens.shape[0]
     seq_total = local_rows * lax.axis_size("sp")
     offset = lax.axis_index("sp") * local_rows
@@ -142,6 +146,455 @@
     return projected.astype(jnp.bfloat16)
 
 
+LANES = 128
+CHUNK = 256
+MESH = pl.DeviceIdType.MESH
+
+
+def rope_tables(offset, rows):
+    half = HEAD // 2
+    inverse = 10000.0 ** (-jnp.arange(half, dtype=jnp.float32) / half)
+    inverse = jnp.tile(inverse, LANES // half)[None, :]
+    sign = jnp.where(jnp.arange(LANES) % HEAD < half, -1.0, 1.0)[None, :]
+    inner = jnp.arange(QB, dtype=jnp.float32)[:, None] * inverse
+    starts = (offset + QB * jnp.arange(rows // QB)).astype(jnp.float32)[:, None] * inverse
+    return jnp.cos(inner), jnp.sin(inner) * sign, jnp.cos(starts), jnp.sin(starts) * sign
+
+
+def mixer_kernel(
+    places, tokens, gain, w_query, kv_block, w_pool, sink, scale, w_out, cos_in, sin_in, cos_at, sin_at,
+    out,
+    tok, normed, wq, wp, kvw, wfull, qs, kv, pool, pool_send, att_send, joined, out_v,
+    tok_sem, own_sem, out_sem, kv_send, kv_recv, kvf_send, wx_send, wx_recv, wo_send, wo_recv,
+    wf_send, wp_send, halo_send, halo_recv, ex_send, ex_recv,
+):
+    S, T = places
+    Z = S // 4
+    s = lax.axis_index("sp")
+    t = lax.axis_index("tp")
+    rows = tokens.shape[0]
+    width = tokens.shape[1]
+    blocks = rows // QB
+    hb = blocks // 2
+    chunks = rows // CHUNK
+    local_heads = w_query.shape[1] // HEAD
+    groups = w_query.shape[1] // LANES
+    pgroups = w_pool.shape[1] // LANES
+    reach = POOL_SPANS[-1] // 2
+    offset = s * rows
+    total_rows = S * rows
+    c = s % 2
+    y = (s // 2) % 2
+    z = s // 4
+    quad = s % 4
+    partner = s + 1 - 2 * c
+    yflip = s + 2 - 4 * y
+    after = (s + 1) % S
+    before = (s + S - 1) % S
+    cross = 1 - t
+    hops = sorted(range(1, Z), key=lambda d: (min(d, Z - d), d))
+
+    def zmate(d, base):
+        return ((z + d) % Z) * 4 + base % 4
+
+    def remote(a, b, send, recv, to_s, to_t):
+        return pltpu.make_async_remote_copy(
+            src_ref=a, dst_ref=b, send_sem=send, recv_sem=recv,
+            device_id={"sp": to_s, "tp": to_t}, device_id_type=MESH,
+        )
+
+    same_core = [zmate(d, s) for d in hops] + [zmate(d, yflip) for d in range(Z)]
+
+    tok_copies = [
+        pltpu.make_async_copy(
+            tokens.at[pl.ds(i * CHUNK, CHUNK)], tok.at[pl.ds(i * CHUNK, CHUNK)], tok_sem.at[i]
+        )
+        for i in range(chunks)
+    ]
+    tok_copies[0].start()
+    own_copies = [
+        pltpu.make_async_copy(w_query, wq, own_sem.at[0]),
+        pltpu.make_async_copy(w_pool, wp, own_sem.at[1]),
+        pltpu.make_async_copy(kv_block, kvw.at[s], own_sem.at[2]),
+        pltpu.make_async_copy(w_out, wfull.at[s, t], own_sem.at[3]),
+    ]
+    for copy in own_copies:
+        copy.start()
+    for copy in tok_copies[1:]:
+        copy.start()
+
+    barrier = pltpu.get_barrier_semaphore()
+    greet = [(b, t) for b in same_core + [after, before]] + [(s, cross)]
+    for to_s, to_t in greet:
+        pl.semaphore_signal(barrier, inc=1, device_id={"sp": to_s, "tp": to_t}, device_id_type=MESH)
+    pl.semaphore_wait(barrier, len(greet))
+
+    kv_copies = [
+        remote(kv_block, kvw.at[s], kv_send.at[i], kv_recv.at[s], b, t)
+        for i, b in enumerate(same_core)
+    ]
+    for copy in kv_copies:
+        copy.start()
+    x_copy = remote(w_out, wfull.at[s, t], wx_send, wx_recv, s, cross)
+    x_copy.start()
+    x_in = remote(w_out, wfull.at[s, cross], wx_send, wx_recv, s, cross)
+
+    kv_forward = [
+        remote(kvw.at[b], kvw.at[b], kvf_send.at[i], kv_recv.at[b], partner, t)
+        for i, b in enumerate([s] + same_core)
+    ]
+    wo_first = [
+        remote(wfull.at[s], wfull.at[s], wo_send.at[i], wo_recv.at[s], b, t)
+        for i, b in enumerate([yflip] + [zmate(d, s) for d in hops] + [partner])
+    ]
+    wo_z = []
+    for i, d in enumerate(hops):
+        b = zmate(d, s)
+        wo_z.append([
+            remote(wfull.at[b], wfull.at[b], wf_send.at[2 * i + k], wo_recv.at[b], to, t)
+            for k, to in enumerate([yflip, partner])
+        ])
+    wo_y = []
+    for i, d in enumerate([0] + hops):
+        b = zmate(d, yflip)
+        wo_y.append(remote(wfull.at[b], wfull.at[b], wp_send.at[i], wo_recv.at[b], partner, t))
+
+    def forward_z(i):
+        wo_z[i][0].wait_recv()
+        wo_z[i][0].start()
+        wo_z[i][1].start()
+
+    def forward_y(i):
+        wo_y[i].wait_recv()
+        wo_y[i].start()
+
+    lane = lax.broadcasted_iota(jnp.int32, (QB, LANES), 1)
+    low_half = lane < HEAD
+    first_half = lane % HEAD < HEAD // 2
+
+    def rotated(values, b):
+        ca = cos_at[pl.ds(b, 1), :]
+        sa = sin_at[pl.ds(b, 1), :]
+        ci = cos_in[...]
+        si = sin_in[...]
+        cosine = ca * ci - sa * si
+        sine = sa * ci + ca * si
+        swapped = jnp.where(
+            first_half,
+            pltpu.roll(values, LANES - HEAD // 2, 1),
+            pltpu.roll(values, HEAD // 2, 1),
+        )
+        return values * cosine + swapped * sine
+
+    own_copies[0].wait()
+    own_copies[1].wait()
+    LN = 32
+
+    def project(i, carry):
+        base = pl.multiple_of(i * CHUNK, CHUNK)
+        pltpu.make_async_copy(
+            tokens.at[pl.ds(base, CHUNK)], tok.at[pl.ds(base, CHUNK)], tok_sem.at[i]
+        ).wait()
+
+        def norm(r, carry):
+            at = pl.multiple_of(base + r * LN, LN)
+            values = tok[pl.ds(at, LN), :].astype(jnp.float32)
+            center = jnp.sum(values, axis=1, keepdims=True) * (1.0 / width)
+            moved = values - center
+            spread = jnp.sum(moved * moved, axis=1, keepdims=True) * (1.0 / width)
+            normed[pl.ds(at, LN), :] = (moved * lax.rsqrt(spread + 1e-06) * gain[...]).astype(
+                jnp.bfloat16
+            )
+            return carry
+
+        lax.fori_loop(0, CHUNK // LN, norm, 0, unroll=2)
+        part = normed[pl.ds(base, CHUNK), :]
+        query = jnp.dot(part, wq[...], preferred_element_type=jnp.float32)
+        for k in range(CHUNK // QB):
+            b = i * (CHUNK // QB) + k
+            for g in range(groups):
+                turned = rotated(query[k * QB:(k + 1) * QB, g * LANES:(g + 1) * LANES], b) * HEAD ** (-0.5)
+                qs[b, pl.ds(2 * g * QB, QB), :] = jnp.where(low_half, turned, 0.0).astype(jnp.bfloat16)
+                qs[b, pl.ds((2 * g + 1) * QB, QB), :] = jnp.where(
+                    low_half, pltpu.roll(turned, HEAD, 1), 0.0
+                ).astype(jnp.bfloat16)
+        mixed = jnp.dot(part, wp[...], preferred_element_type=jnp.float32)
+        pool[pl.ds(pl.multiple_of(reach + base, 8), CHUNK), :] = mixed.astype(jnp.bfloat16).astype(jnp.float32)
+
+        @pl.when(i == 1)
+        def _():
+            own_copies[3].wait()
+            x_in.wait_recv()
+            for copy in wo_first:
+                copy.start()
+
+        @pl.when(i == 2)
+        def _():
+            own_copies[2].wait()
+            for copy in kv_forward[1:]:
+                copy.wait_recv()
+            for copy in kv_forward:
+                copy.start()
+        return carry
+
+    lax.fori_loop(0, chunks, project, 0)
+
+    halo_pool = [
+        remote(pool.at[pl.ds(rows, reach)], pool.at[pl.ds(0, reach)], halo_send.at[0], halo_recv.at[0], after, t),
+        remote(pool.at[pl.ds(reach, reach)], pool.at[pl.ds(rows + reach, reach)], halo_send.at[1], halo_recv.at[1], before, t),
+    ]
+    halo_kv = [
+        remote(kv.at[pl.ds(rows, WINDOW)], kv.at[pl.ds(0, WINDOW)], halo_send.at[2], halo_recv.at[2], after, t),
+        remote(kv.at[pl.ds(WINDOW, WINDOW)], kv.at[pl.ds(rows + WINDOW, WINDOW)], halo_send.at[3], halo_recv.at[3], before, t),
+    ]
+
+    for b in [partner] + [zmate(d, partner) for d in hops] + [zmate(d, partner + 2 - 4 * y) for d in range(Z)]:
+        remote(kvw.at[b], kvw.at[b], kvf_send.at[0], kv_recv.at[b], partner, t).wait_recv()
+
+    def key_value(j, carry):
+        i = jnp.where(j == 0, 0, jnp.where(j == 1, chunks - 1, j - 1))
+        base = pl.multiple_of(i * CHUNK, CHUNK)
+        both = jnp.dot(
+            normed[pl.ds(base, CHUNK), :], kvw[...].reshape(width, LANES), preferred_element_type=jnp.float32
+        )
+        for k in range(CHUNK // QB):
+            piece = both[k * QB:(k + 1) * QB, :]
+            turned = rotated(piece, i * (CHUNK // QB) + k)
+            kv[pl.ds(pl.multiple_of(WINDOW + base + k * QB, QB), QB), :] = jnp.where(
+                low_half, turned, piece
+            ).astype(jnp.bfloat16)
+
+        @pl.when(j == 0)
+        def _():
+            for copy in halo_pool:
+                copy.start()
+
+        @pl.when(j == 2)
+        def _():
+            for copy in halo_kv:
+                copy.start()
+        return carry
+
+    lax.fori_loop(0, chunks, key_value, 0)
+
+    for copy in halo_pool:
+        copy.wait_recv()
+
+    @pl.when(s == 0)
+    def _():
+        pool[0:reach, :] = jnp.zeros((reach, pool.shape[1]), jnp.float32)
+
+    @pl.when(s == S - 1)
+    def _():
+        pool[rows + reach:rows + 2 * reach, :] = jnp.zeros((reach, pool.shape[1]), jnp.float32)
+
+    def pooled(b, g):
+        cols = slice(g * LANES, (g + 1) * LANES)
+        length = QB + 2 * reach
+        values = pool[pl.ds(pl.multiple_of(b * QB, QB), length), cols]
+        index = (t * (pgroups * LANES) + g * LANES) // POOL_CH
+        running = values
+        stride = 1
+        picked = jnp.zeros((QB, LANES), jnp.float32)
+        wide = 0
+        for k, span in enumerate(POOL_SPANS):
+            running = running + pltpu.roll(running, length - stride, 0)
+            stride = span
+            shift = reach - span // 2
+            sums = (pltpu.roll(running, length - shift, 0) if shift else running)[:QB]
+            picked = jnp.where(index == k, sums, picked)
+            wide = jnp.where(index == k, span // 2, wide)
+        pos = offset + b * QB + lax.broadcasted_iota(jnp.int32, (QB, LANES), 0)
+        counted = (jnp.minimum(pos + wide, total_rows) - jnp.maximum(pos - wide, 0)).astype(jnp.float32)
+        return ((picked / counted - values[reach:reach + QB]) * scale[:, cols]).astype(jnp.bfloat16)
+
+    def pool_other(i, carry):
+        for g in range(pgroups):
+            pool_send[pl.ds(pl.multiple_of(i * QB, QB), QB), g * LANES:(g + 1) * LANES] = pooled(cross * hb + i, g)
+        return carry
+
+    def pool_own(i, carry):
+        for g in range(pgroups):
+            joined[T + t, pl.ds(pl.multiple_of(i * QB, QB), QB), g * LANES:(g + 1) * LANES] = pooled(t * hb + i, g)
+        return carry
+
+    ex_pool = remote(pool_send, joined.at[T + t], ex_send.at[0], ex_recv.at[0], s, cross)
+    ex_att = remote(att_send, joined.at[t], ex_send.at[1], ex_recv.at[1], s, cross)
+    lax.fori_loop(0, hb, pool_other, 0)
+    lax.fori_loop(0, hb, pool_own, 0)
+    ex_pool.start()
+    for i in range(min(2, len(hops))):
+        forward_z(i)
+
+    span = QB + 2 * WINDOW
+    row_id = lax.broadcasted_iota(jnp.int32, (QB, span), 0)
+    col_id = lax.broadcasted_iota(jnp.int32, (QB, span), 1)
+
+    def attend(b):
+        context = kv[pl.ds(pl.multiple_of(b * QB, QB), span), :]
+        scores = lax.dot_general(
+            qs[b], context, (((1,), (1,)), ((), ())), preferred_element_type=jnp.float32
+        )
+        start = offset + b * QB
+        lowest = jnp.maximum(row_id, WINDOW - start)
+        highest_col = jnp.minimum(row_id + 2 * WINDOW, total_rows - 1 - start + WINDOW)
+        valid = (col_id >= lowest) & (col_id <= highest_col)
+        expos = []
+        norms = []
+        for h in range(local_heads):
+            part = jnp.where(valid, scores[h * QB:(h + 1) * QB], NEG_BIG)
+            top = jnp.maximum(jnp.max(part, axis=1, keepdims=True), sink[h])
+            expo = jnp.exp(part - top)
+            norms.append(1.0 / (jnp.sum(expo, axis=1, keepdims=True) + jnp.exp(sink[h] - top)))
+            expos.append(expo.astype(jnp.bfloat16))
+        result = jnp.dot(jnp.concatenate(expos, axis=0), context, preferred_element_type=jnp.float32)
+        heads = [result[h * QB:(h + 1) * QB] * norms[h] for h in range(local_heads)]
+        return [
+            jnp.where(low_half, pltpu.roll(heads[2 * g], HEAD, 1), heads[2 * g + 1]).astype(jnp.bfloat16)
+            for g in range(groups)
+        ]
+
+    def attend_other(i, carry):
+        @pl.when(i == hb - 1)
+        def _():
+            halo_kv[0].wait_recv()
+            halo_kv[1].wait_recv()
+        b = jnp.where(t == 0, hb + i, hb - 1 - i)
+        at = pl.multiple_of((b - cross * hb) * QB, QB)
+        for g, value in enumerate(attend(b)):
+            att_send[pl.ds(at, QB), g * LANES:(g + 1) * LANES] = value
+        return carry
+
+    def attend_own(i, carry):
+        b = jnp.where(t == 0, hb - 1 - i, hb + i)
+        at = pl.multiple_of((b - t * hb) * QB, QB)
+        for g, value in enumerate(attend(b)):
+            joined[t, pl.ds(at, QB), g * LANES:(g + 1) * LANES] = value
+
+        @pl.when(i == 0)
+        def _():
+            ex_att.start()
+        return carry
+
+    lax.fori_loop(0, hb, attend_other, 0)
+    forward_y(0)
+    for i in range(2, len(hops)):
+        forward_z(i)
+    lax.fori_loop(0, hb, attend_own, 0)
+    for i in range(1, Z):
+        forward_y(i)
+
+    remote(pool_send, joined.at[T + cross], ex_send.at[0], ex_recv.at[0], s, cross).wait_recv()
+    remote(att_send, joined.at[cross], ex_send.at[1], ex_recv.at[1], s, cross).wait_recv()
+    for base_place in (partner, partner + 2 - 4 * y):
+        for d in [0] + hops:
+            b = zmate(d, base_place)
+            remote(wfull.at[b], wfull.at[b], wp_send.at[0], wo_recv.at[b], partner, t).wait_recv()
+
+    def out_copy(n):
+        return pltpu.make_async_copy(
+            out_v.at[n], out.at[:, pl.ds(pl.multiple_of(n * 2 * LANES, 2 * LANES), 2 * LANES)], out_sem.at[n]
+        )
+
+    def finish(n, carry):
+        left = jnp.concatenate([joined[k] for k in range(2 * T)], axis=1)
+        right = jnp.concatenate(
+            [wfull[2 * n].reshape(left.shape[1], LANES), wfull[2 * n + 1].reshape(left.shape[1], LANES)], axis=1
+        )
+        out_v[n] = jnp.dot(left, right, preferred_element_type=jnp.float32).astype(jnp.bfloat16)
+        out_copy(n).start()
+        return carry
+
+    lax.fori_loop(0, S // 2, finish, 0)
+    for copy in kv_copies + [x_copy] + kv_forward + wo_first + wo_y + halo_pool + halo_kv + [ex_pool, ex_att]:
+        copy.wait_send()
+    for pair in wo_z:
+        for copy in pair:
+            copy.wait_send()
+    for n in range(S // 2):
+        out_copy(n).wait()
+
+
+def body(mesh, tokens, norm_gain, w_query, w_key, w_value, w_pool_in, sink_logit, pool_scale, w_out):
+    S = lax.axis_size("sp")
+    T = lax.axis_size("tp")
+    rows, width = tokens.shape
+    local_heads = w_query.shape[1] // HEAD
+    fits = (
+        S % 4 == 0 and S > 4 and T == 2
+        and w_out.shape[1] == LANES and w_key.shape[0] == LANES
+        and w_query.shape[1] % LANES == 0 and w_pool_in.shape[1] % LANES == 0
+        and w_query.shape[1] == w_pool_in.shape[1]
+        and local_heads == QH // KVH and rows % (2 * CHUNK) == 0
+    )
+    if not fits:
+        return plain_body(
+            tokens, norm_gain, w_query, w_key, w_value, w_pool_in, sink_logit, pool_scale, w_out
+        )
+    place = lax.axis_index("tp")
+    key_head = place * local_heads // (QH // KVH)
+    kv_block = jnp.concatenate(
+        [
+            lax.dynamic_slice_in_dim(w_key, key_head * HEAD, HEAD, 1),
+            lax.dynamic_slice_in_dim(w_value, key_head * HEAD, HEAD, 1),
+        ],
+        axis=1,
+    )
+    tables = rope_tables(lax.axis_index("sp") * rows, rows)
+    blocks = rows // QB
+    half = rows // T
+    Z = S // 4
+    reach = POOL_SPANS[-1] // 2
+    wide = w_query.shape[1]
+    vmem = pl.BlockSpec(memory_space=pltpu.VMEM)
+    smem = pl.BlockSpec(memory_space=pltpu.SMEM)
+    hbm = pl.BlockSpec(memory_space=pl.ANY)
+    dma = pltpu.SemaphoreType.DMA
+    bf = jnp.bfloat16
+    return pl.pallas_call(
+        functools.partial(mixer_kernel, (S, T)),
+        out_shape=jax.ShapeDtypeStruct((half, S * w_out.shape[1]), bf),
+        in_specs=[hbm, vmem, hbm, hbm, hbm, smem, vmem, hbm, vmem, vmem, vmem, vmem],
+        out_specs=hbm,
+        scratch_shapes=[
+            pltpu.VMEM((rows, width), bf),
+            pltpu.VMEM((rows, width), bf),
+            pltpu.VMEM(w_query.shape, bf),
+            pltpu.VMEM(w_pool_in.shape, bf),
+            pltpu.VMEM((S, LANES, LANES), bf),
+            pltpu.VMEM((S, T) + w_out.shape, bf),
+            pltpu.VMEM((blocks, local_heads * QB, LANES), bf),
+            pltpu.VMEM((rows + 2 * WINDOW, LANES), bf),
+            pltpu.VMEM((rows + 2 * reach, wide), jnp.float32),
+            pltpu.VMEM((half, wide), bf),
+            pltpu.VMEM((half, wide), bf),
+            pltpu.VMEM((2 * T, half, wide), bf),
+            pltpu.VMEM((S // 2, half, 2 * LANES), bf),
+            dma((rows // CHUNK,)),
+            dma((4,)),
+            dma((S // 2,)),
+            dma((S // 2 - 1,)),
+            dma((S,)),
+            dma((S // 2,)),
+            dma(()),
+            dma(()),
+            dma((Z + 1,)),
+            dma((S,)),
+            dma((2 * (Z - 1),)),
+            dma((Z,)),
+            dma((4,)),
+            dma((4,)),
+            dma((2,)),
+            dma((2,)),
+        ],
+        compiler_params=pltpu.CompilerParams(
+            collective_id=0, has_side_effects=True, vmem_limit_bytes=44 * 1024 * 1024
+        ),
+    )(
+        tokens, norm_gain[None, :], w_query, kv_block, w_pool_in, sink_logit, pool_scale[None, :], w_out, *tables
+    )
+
+
 def solution(mesh):
     in_specs = (
         P("sp", None),
@@ -155,4 +608,4 @@
         P("tp", "sp"),
     )
     out_specs = P(("sp", "tp"), None)
-    return jax.shard_map(body, mesh=mesh, in_specs=in_specs, out_specs=out_specs, check_vma=False)
+    return jax.shard_map(functools.partial(body, mesh), mesh=mesh, in_specs=in_specs, out_specs=out_specs, check_vma=False)

time: 168 us -> 65 us (0.39)
  the two profiles are of different devices: /device:TPU:0 before, /device:TPU:9 now
where the time goes in v1:
time: 65 us; the launch traced here: 63.8 us
  Pallas kernels  53.4 us (82%)
  local copies, waits for them, and re-layouts  9.84 us (15%)
    pallas_call x1, Pallas kernels, body(): pl.pallas_call(functools.partial(mixer_kernel, (S, T)), out_shape=jax.Sha...  53.4 us
    unnamed x15, local copies, waits for them, and re-layouts  8.89 us

profile of v1, /device:TPU:9, one launch (start us, length us, event | category | flops | bytes accessed | tf_op | source)
XLA Modules:
  0.0 63.8 jit_solution(3379712622910780878)
XLA Ops:
  0.0 0.1 mul.74
  0.1 0.1 fusion.1
  0.2 0.9 %constant_dynamic-slice_fusion = (bf16[128,64]{1,0:T(8,128)(2,1)S(1)}, bf16[128,64]{1,0:T(8,128)(2,1)S(1)}) fusion(bf16[128,128]{1,0:T(8,128)(2,1)} %param.13, s32[]{:T(128)S(6)} %select_n.32, bf16[128,128]{1,0:T(8,128)(2,1)} %param.12), kind=kLoop, calls=%fused_computation.11 | loop fusion | bytes 65540 | tf_op jit(solution)/shard_map/dynamic_slice | solution.py:539
  1.1 0.1 pad_maximum_fusion.kv_block
  1.2 0.3 sine_multiply_fusion
  1.5 0.0 copy-start
  1.5 2.2 %copy-done = bf16[1024,2048]{1,0:T(8,128)(2,1)S(1)} copy-done((bf16[1024,2048]{1,0:T(8,128)(2,1)S(1)}, bf16[1024,2048]{1,0:T(8,128)(2,1)}, u32[]{:S(2)}) %copy-start) | copy-done | bytes 4194328
  3.7 0.0 copy-start.1
  3.7 1.2 %copy-done.1 = bf16[2048,256]{1,0:T(8,128)(2,1)S(1)} copy-done((bf16[2048,256]{1,0:T(8,128)(2,1)S(1)}, bf16[2048,256]{1,0:T(8,128)(2,1)}, u32[]{:S(2)}) %copy-start.1) | copy-done | bytes 1048600
  4.9 0.0 copy-start.2
  4.9 1.2 %copy-done.2 = bf16[2048,256]{1,0:T(8,128)(2,1)S(1)} copy-done((bf16[2048,256]{1,0:T(8,128)(2,1)S(1)}, bf16[2048,256]{1,0:T(8,128)(2,1)}, u32[]{:S(2)}) %copy-start.2) | copy-done | bytes 1048600
  6.1 0.0 copy-start.3
  6.1 0.9 %copy-done.3 = bf16[512,128]{1,0:T(8,128)(2,1)S(1)} copy-done((bf16[512,128]{1,0:T(8,128)(2,1)S(1)}, bf16[512,128]{1,0:T(8,128)(2,1)}, u32[]{:S(2)}) %copy-start.3) | copy-done | bytes 131096
  7.0 0.0 copy-start.4
  7.0 0.7 %copy-done.4 = f32[2048]{0:T(1024)S(1)} copy-done((f32[2048]{0:T(1024)S(1)}, f32[2048]{0:T(1024)}, u32[]{:S(2)}) %copy-start.4) | copy-done | bytes 8216
  7.7 0.0 copy-start.5
  7.7 0.7 %copy-done.5 = f32[256]{0:T(256)S(1)} copy-done((f32[256]{0:T(256)S(1)}, f32[256]{0:T(256)}, u32[]{:S(2)}) %copy-start.5) | copy-done | bytes 1048
  8.4 0.0 copy-start.6
  8.4 0.7 %copy-done.6 = f32[4]{0:T(128)S(1)} copy-done((f32[4]{0:T(128)S(1)}, f32[4]{0:T(128)}, u32[]{:S(2)}) %copy-start.6) | copy-done | bytes 40
  9.0 53.4 %shard_map.91 = bf16[512,2048]{1,0:T(8,128)(2,1)S(1)} custom-call(bf16[1024,2048]{1,0:T(8,128)(2,1)S(1)} %copy-done, f32[1,2048]{1,0:T(1,128)S(1)} %bitcast.2, bf16[2048,256]{1,0:T(8,128)(2,1)S(1)} %copy-done.1, bf16[128,128]{1,0:T(8,128)(2,1)S(1)} %pad_maximum_fusion.kv_block, bf16[2048,256]{1,0:T(8,128)(2,1)S(1)} %copy-done.2, f32[4]{0:T(128)S(1)} %copy-done.6, ...), custom_call_target="tpu_custom_call" | custom-call | tf_op jit(solution)/shard_map/pallas_call | solution.py:554
  62.5 1.3 %copy.11 = bf16[512,2048]{1,0:T(8,128)(2,1)} copy(bf16[512,2048]{1,0:T(8,128)(2,1)S(1)} %shard_map.91) | data formatting | bytes 4194304
  (4 shorter events, 0.0 us)
Async XLA Ops:
  1.5 2.2 %copy-start = (bf16[1024,2048]{1,0:T(8,128)(2,1)S(1)}, bf16[1024,2048]{1,0:T(8,128)(2,1)}, u32[]{:S(2)}) copy-start(bf16[1024,2048]{1,0:T(8,128)(2,1)} %tokens.1) | copy-start | bytes 12582916
  3.7 1.2 %copy-start.1 = (bf16[2048,256]{1,0:T(8,128)(2,1)S(1)}, bf16[2048,256]{1,0:T(8,128)(2,1)}, u32[]{:S(2)}) copy-start(bf16[2048,256]{1,0:T(8,128)(2,1)} %w_query.1) | copy-start | bytes 3145732
  4.9 1.2 %copy-start.2 = (bf16[2048,256]{1,0:T(8,128)(2,1)S(1)}, bf16[2048,256]{1,0:T(8,128)(2,1)}, u32[]{:S(2)}) copy-start(bf16[2048,256]{1,0:T(8,128)(2,1)} %w_pool.1) | copy-start | bytes 3145732
  6.1 0.9 %copy-start.3 = (bf16[512,128]{1,0:T(8,128)(2,1)S(1)}, bf16[512,128]{1,0:T(8,128)(2,1)}, u32[]{:S(2)}) copy-start(bf16[512,128]{1,0:T(8,128)(2,1)} %w_out.1) | copy-start | bytes 393220
  7.0 0.7 %copy-start.4 = (f32[2048]{0:T(1024)S(1)}, f32[2048]{0:T(1024)}, u32[]{:S(2)}) copy-start(f32[2048]{0:T(1024)} %param.10) | copy-start | bytes 24580
  7.7 0.7 %copy-start.5 = (f32[256]{0:T(256)S(1)}, f32[256]{0:T(256)}, u32[]{:S(2)}) copy-start(f32[256]{0:T(256)} %param.16) | copy-start | bytes 3076
  8.4 0.7 %copy-start.6 = (f32[4]{0:T(128)S(1)}, f32[4]{0:T(128)}, u32[]{:S(2)}) copy-start(f32[4]{0:T(128)} %sink.1) | copy-start | bytes 52

commit v2 on v1

--- a/solution.py
+++ b/solution.py
@@ -243,30 +243,43 @@
         remote(kvw.at[b], kvw.at[b], kvf_send.at[i], kv_recv.at[b], partner, t)
         for i, b in enumerate([s] + same_core)
     ]
-    wo_first = [
-        remote(wfull.at[s], wfull.at[s], wo_send.at[i], wo_recv.at[s], b, t)
-        for i, b in enumerate([yflip] + [zmate(d, s) for d in hops] + [partner])
-    ]
-    wo_z = []
-    for i, d in enumerate(hops):
-        b = zmate(d, s)
-        wo_z.append([
-            remote(wfull.at[b], wfull.at[b], wf_send.at[2 * i + k], wo_recv.at[b], to, t)
-            for k, to in enumerate([yflip, partner])
-        ])
-    wo_y = []
-    for i, d in enumerate([0] + hops):
+    wo_to = [zmate(d, s) for d in hops] + [yflip, partner]
+    wo_own = [
+        remote(w_out, wfull.at[s, t], wo_send.at[0, i], wo_recv.at[s, t], b, t)
+        for i, b in enumerate(wo_to)
+    ]
+    wo_crossed = [
+        remote(wfull.at[s, cross], wfull.at[s, cross], wo_send.at[1, i], wo_recv.at[s, cross], b, t)
+        for i, b in enumerate(wo_to)
+    ]
+    for copy in wo_own:
+        copy.start()
+
+    def z_copies(i, k):
+        b = zmate(hops[i], s)
+        half = cross if k else t
+        piece = wfull.at[b, half]
+        return [
+            remote(piece, piece, wf_send.at[k, 2 * i + j], wo_recv.at[b, half], to, t)
+            for j, to in enumerate([yflip, partner])
+        ]
+
+    def y_copy(d, k):
         b = zmate(d, yflip)
-        wo_y.append(remote(wfull.at[b], wfull.at[b], wp_send.at[i], wo_recv.at[b], partner, t))
-
-    def forward_z(i):
-        wo_z[i][0].wait_recv()
-        wo_z[i][0].start()
-        wo_z[i][1].start()
-
-    def forward_y(i):
-        wo_y[i].wait_recv()
-        wo_y[i].start()
+        half = cross if k else t
+        piece = wfull.at[b, half]
+        return remote(piece, piece, wp_send.at[k, d], wo_recv.at[b, half], partner, t)
+
+    def forward_z(i, k):
+        copies = z_copies(i, k)
+        copies[0].wait_recv()
+        for copy in copies:
+            copy.start()
+
+    def forward_y(d, k):
+        copy = y_copy(d, k)
+        copy.wait_recv()
+        copy.start()
 
     lane = lax.broadcasted_iota(jnp.int32, (QB, LANES), 1)
     low_half = lane < HEAD
@@ -321,11 +334,10 @@
         mixed = jnp.dot(part, wp[...], preferred_element_type=jnp.float32)
         pool[pl.ds(pl.multiple_of(reach + base, 8), CHUNK), :] = mixed.astype(jnp.bfloat16).astype(jnp.float32)
 
-        @pl.when(i == 1)
+        @pl.when(i == 0)
         def _():
-            own_copies[3].wait()
             x_in.wait_recv()
-            for copy in wo_first:
+            for copy in wo_crossed:
                 copy.start()
 
         @pl.when(i == 2)
@@ -423,8 +435,8 @@
     lax.fori_loop(0, hb, pool_other, 0)
     lax.fori_loop(0, hb, pool_own, 0)
     ex_pool.start()
-    for i in range(min(2, len(hops))):
-        forward_z(i)
+    for i in range(len(hops)):
+        forward_z(i, 0)
 
     span = QB + 2 * WINDOW
     row_id = lax.broadcasted_iota(jnp.int32, (QB, span), 0)
@@ -477,26 +489,30 @@
         return carry
 
     lax.fori_loop(0, hb, attend_other, 0)
-    forward_y(0)
-    for i in range(2, len(hops)):
-        forward_z(i)
     lax.fori_loop(0, hb, attend_own, 0)
-    for i in range(1, Z):
-        forward_y(i)
+    for i in range(len(hops)):
+        forward_z(i, 1)
+    for d in range(Z):
+        forward_y(d, 0)
+    own_copies[3].wait()
 
     remote(pool_send, joined.at[T + cross], ex_send.at[0], ex_recv.at[0], s, cross).wait_recv()
     remote(att_send, joined.at[cross], ex_send.at[1], ex_recv.at[1], s, cross).wait_recv()
-    for base_place in (partner, partner + 2 - 4 * y):
-        for d in [0] + hops:
-            b = zmate(d, base_place)
-            remote(wfull.at[b], wfull.at[b], wp_send.at[0], wo_recv.at[b], partner, t).wait_recv()
-
     def out_copy(n):
         return pltpu.make_async_copy(
             out_v.at[n], out.at[:, pl.ds(pl.multiple_of(n * 2 * LANES, 2 * LANES), 2 * LANES)], out_sem.at[n]
         )
 
-    def finish(n, carry):
+    def finish(j, carry):
+        over = j // Z
+        @pl.when(over == 0)
+        def _():
+            forward_y(j, 1)
+        side = y + over - 2 * y * over
+        n = ((z + j) % Z) * 2 + side
+        for half in range(T):
+            piece = wfull.at[2 * n + 1 - c, half]
+            remote(piece, piece, wp_send.at[0, 0], wo_recv.at[2 * n + 1 - c, half], partner, t).wait_recv()
         left = jnp.concatenate([joined[k] for k in range(2 * T)], axis=1)
         right = jnp.concatenate(
             [wfull[2 * n].reshape(left.shape[1], LANES), wfull[2 * n + 1].reshape(left.shape[1], LANES)], axis=1
@@ -506,11 +522,14 @@
         return carry
 
     lax.fori_loop(0, S // 2, finish, 0)
-    for copy in kv_copies + [x_copy] + kv_forward + wo_first + wo_y + halo_pool + halo_kv + [ex_pool, ex_att]:
+    for copy in kv_copies + [x_copy] + kv_forward + wo_own + wo_crossed + halo_pool + halo_kv + [ex_pool, ex_att]:
         copy.wait_send()
-    for pair in wo_z:
-        for copy in pair:
-            copy.wait_send()
+    for k in range(2):
+        for i in range(len(hops)):
+            for copy in z_copies(i, k):
+                copy.wait_send()
+        for d in range(Z):
+            y_copy(d, k).wait_send()
     for n in range(S // 2):
         out_copy(n).wait()
 
@@ -578,17 +597,17 @@
             dma((S // 2,)),
             dma(()),
             dma(()),
-            dma((Z + 1,)),
-            dma((S,)),
-            dma((2 * (Z - 1),)),
-            dma((Z,)),
+            dma((T, Z + 1)),
+            dma((S, T)),
+            dma((T, 2 * (Z - 1))),
+            dma((T, Z)),
             dma((4,)),
             dma((4,)),
             dma((2,)),
             dma((2,)),
         ],
         compiler_params=pltpu.CompilerParams(
-            collective_id=0, has_side_effects=True, vmem_limit_bytes=44 * 1024 * 1024
+            collective_id=0, has_side_effects=True, vmem_limit_bytes=62 * 1024 * 1024
         ),
     )(
         tokens, norm_gain[None, :], w_query, kv_block, w_pool_in, sink_logit, pool_scale[None, :], w_out, *tables

time: 65 us -> 58.6 us (0.902); the launches traced: 63.8 us -> 58.3 us
  local copies, waits for them, and re-layouts: 9.84 us -> 4.11 us
  other arithmetic: 0.48 us -> 2.35 us
  Pallas kernels: 53.4 us -> 51.8 us
    unnamed x15 -> x1, local copies, waits for them, and re-layouts: 8.89 us -> 3.16 us
    pallas_call x1, Pallas kernels: 53.4 us -> 51.8 us  [body(): pl.pallas_call(functools.partial(mixer_kernel, (S, T)), out_shape=jax.Sha...]
    mul x1, other arithmetic: 0.26 us -> 0.91 us  [rope_tables(): jnp.sin(inner) * sign]
where the time goes in v2:
time: 58.6 us; the launch traced here: 58.3 us
  Pallas kernels  51.8 us (88%)
  local copies, waits for them, and re-layouts  4.11 us (7%)
  other arithmetic  2.35 us (4%)
    pallas_call x1, Pallas kernels, body(): pl.pallas_call(functools.partial(mixer_kernel, (S, T)), out_shape=jax.Sha...  51.8 us
    unnamed x1, local copies, waits for them, and re-layouts  3.16 us

profile of v2, /device:TPU:9, one launch (start us, length us, event | category | flops | bytes accessed | tf_op | source)
XLA Modules:
  0.0 58.3 jit_solution(9687799489161220409)
XLA Ops:
  0.0 0.1 mul.74
  0.1 0.7 %fusion.1 = (f32[8,128]{1,0:T(8,128)}, f32[8,128]{1,0:T(8,128)}) fusion(f32[128]{0:T(128)S(1)} %compare_select_fusion, f32[128]{0:T(128)S(1)} %mul.74, f32[8]{0:T(128)S(1)} %add_convert_fusion), kind=kLoop, calls=%fused_computation.6 | loop fusion | flops 2048 | bytes 9248 | tf_op jit(solution)/shard_map/mul | solution.py:161
  0.8 0.9 %constant_dynamic-slice_fusion = (bf16[128,64]{1,0:T(8,128)(2,1)S(1)}, bf16[128,64]{1,0:T(8,128)(2,1)S(1)}) fusion(bf16[128,128]{1,0:T(8,128)(2,1)} %param.13, s32[]{:T(128)S(6)} %select_n.32, bf16[128,128]{1,0:T(8,128)(2,1)} %param.12), kind=kLoop, calls=%fused_computation.11 | loop fusion | bytes 65540 | tf_op jit(solution)/shard_map/dynamic_slice | solution.py:558
  1.7 0.7 %pad_maximum_fusion.kv_block = bf16[128,128]{1,0:T(8,128)(2,1)} fusion(bf16[128,64]{1,0:T(8,128)(2,1)S(1)} %get-tuple-element.9, bf16[128,64]{1,0:T(8,128)(2,1)S(1)} %get-tuple-element.10), kind=kLoop, calls=%fused_computation.3 | loop fusion | flops 65536 | bytes 65536 | tf_op jit(solution)/shard_map/concatenate | solution.py:555
  2.4 0.9 %sine_multiply_fusion = (f32[128,128]{1,0:T(8,128)}, f32[128,128]{1,0:T(8,128)}) fusion(f32[128]{0:T(128)S(1)} %compare_select_fusion, f32[128]{0:T(128)S(1)} %mul.74), kind=kLoop, calls=%fused_computation | loop fusion | flops 32768 | bytes 132096 | tf_op jit(solution)/shard_map/mul | solution.py:161
  3.3 51.8 %shard_map.91 = bf16[512,2048]{1,0:T(8,128)(2,1)} custom-call(bf16[1024,2048]{1,0:T(8,128)(2,1)} %tokens.1, f32[1,2048]{1,0:T(1,128)} %bitcast.2, bf16[2048,256]{1,0:T(8,128)(2,1)} %w_query.1, bf16[128,128]{1,0:T(8,128)(2,1)} %pad_maximum_fusion.kv_block, bf16[2048,256]{1,0:T(8,128)(2,1)} %w_pool.1, f32[4]{0:T(128)} %sink.1, f32[1,256]{1,0:T(1,128)} %bitcast.3, ...), custom_call_target="tpu_custom_call" | custom-call | tf_op jit(solution)/shard_map/pallas_call | solution.py:573
  55.2 3.2 %copy.11 = bf16[512,2048]{1,0:T(8,128)(2,1)} copy(bf16[512,2048]{1,0:T(8,128)(2,1)} %shard_map.91) | data formatting | bytes 4194304
  (4 shorter events, 0.0 us)
